TPU v7x, 32 devices: a whole 2x2x4 slice. The times are simulated.
32 devices in a mesh: sp: 8 (over z, x), tp: 4 (over y, core).
Axes of the slice: x: 2, y: 2, z: 4, core: 2. Of those that a mesh axis runs over, the one named last changes fastest.
Arguments:
- resid: bfloat16 [2048, 2048], P('sp'), may hold values from -6 to 6
- query_one: bfloat16 [2048, 1024], P('sp', 'tp'), may hold values from -400 to 400
- query_two: bfloat16 [2048, 1024], P('sp', 'tp'), may hold values from -400 to 400
- key_one: bfloat16 [2048, 1024], P('sp', 'tp'), may hold values from -8 to 8
- key_two: bfloat16 [2048, 1024], P('sp', 'tp'), may hold values from -8 to 8
- values: bfloat16 [2048, 2048], P('sp', 'tp'), may hold values from -6 to 6
- documents: int32 [2048], P('sp'), may hold values from 0 to 1, never falling along the last dimension, each value on 1 to 1280 neighbouring positions
- mix_lambda: float32 [16], P('tp'), may hold values from 0.3 to 0.8
- head_gain: float32 [128], replicated, may hold values from 0.1 to 1.9
- out_weight: bfloat16 [2048, 2048], P('tp'), may hold values from -0.125 to 0.125
- ffn_gain: float32 [2048], replicated, may hold values from 0.1 to 1.9
- routes: int32 [2048, 4], P('sp'), may hold values from 0 to 31, all different within a row; in each aligned block of 256 rows (0 to 255, 256 to 511, ...) at most 64 rows name the same one
- route_weight: float32 [2048, 4], P('sp'), may hold values from 0.2 to 0.9
- expert_gate: bfloat16 [32, 2048, 512], P(('sp', 'tp')), may hold values from -0.125 to 0.125
- expert_up: bfloat16 [32, 2048, 512], P(('sp', 'tp')), may hold values from -0.125 to 0.125
- expert_down: bfloat16 [32, 512, 2048], P(('sp', 'tp')), may hold values from -0.25 to 0.25
- shared_gate: bfloat16 [2048, 512], P(None, 'tp'), may hold values from -0.125 to 0.125
- shared_up: bfloat16 [2048, 512], P(None, 'tp'), may hold values from -0.125 to 0.125
- shared_down: bfloat16 [512, 2048], P('tp'), may hold values from -0.25 to 0.25
Outputs:
- layer_out: bfloat16 [2048, 2048], P(('sp', 'tp'))
Inputs may be any that keep to these rules, and one draw needn't show every extreme that they name: `documents`: document numbers never fall along the positions; each document has 1 to 1280 positions and one has exactly 1280. `routes`: A row names 4 different experts. In each aligned block of 256 rows no expert is named by more than 64 rows, a bound that some block reaches.
All inputs are finite; a program needn't handle non-finite values.
Results may differ from a plain program's by a relative error of at most 0.018.
Values may be sent and summed in bfloat16 or wider, within the bound.
A program may use at most 128 MiB of HBM per device.

v0:
```python
import jax
import jax.numpy as jnp
from jax import lax
from jax.sharding import PartitionSpec as P

NEG_FILL = -1e30
HEAD_SCALE = 0.8


def rms_scale(values_in, eps_value):
    return lax.rsqrt(jnp.mean(values_in * values_in, axis=-1, keepdims=True) + eps_value)


def local(
    resid,
    query_one,
    query_two,
    key_one,
    key_two,
    values,
    documents,
    mix_lambda,
    head_gain,
    out_weight,
    ffn_gain,
    routes,
    route_weight,
    expert_gate,
    expert_up,
    expert_down,
    shared_gate,
    shared_up,
    shared_down,
):
    tok_rows = query_one.shape[0]
    head_count = mix_lambda.shape[0]
    head_width = query_one.shape[1] // head_count
    value_width = values.shape[1] // head_count
    model_width = resid.shape[1]
    score_scale = head_width ** (-0.5)
    seq_size = lax.axis_size("sp")
    tp_size = lax.axis_size("tp")
    query_pos = lax.axis_index("sp") * tok_rows + jnp.arange(tok_rows, dtype=jnp.int32)
    query_first = query_one.reshape(tok_rows, head_count, head_width)
    query_second = query_two.reshape(tok_rows, head_count, head_width)
    lambda_col = mix_lambda[:, None, None]
    first_doc = documents[0]
    last_pos = query_pos[tok_rows - 1]

    def masks(key_docs):
        key_pos = jnp.arange(key_docs.shape[0], dtype=jnp.int32)
        return (
            (key_pos[None, :] <= query_pos[:, None]) & (key_docs[None, :] == documents[:, None])
        )[None]

    def needed(key_docs, offset):
        return (offset <= last_pos) & (jnp.max(key_docs) >= first_doc)

    def scores(query_block, key_block):
        keyed = key_block.reshape(key_block.shape[0], head_count, head_width)
        return (
            jnp.einsum("qhd,khd->hqk", query_block, keyed, preferred_element_type=jnp.float32)
            * score_scale
        )

    empty_max = jnp.full((head_count, tok_rows), NEG_FILL, jnp.float32)
    empty_sum = jnp.zeros((head_count, tok_rows), jnp.float32)
    stats_init = ((empty_max, empty_sum), (empty_max, empty_sum))
    value_init = jnp.zeros((head_count, tok_rows, value_width), jnp.float32)
    key_first = lax.all_gather(key_one, "sp", axis=0, tiled=True)
    key_second = lax.all_gather(key_two, "sp", axis=0, tiled=True)
    key_docs = lax.all_gather(documents, "sp", axis=0, tiled=True)

    def stats_update(current):
        allowed = masks(key_docs)
        result = []
        for query_block, key_block, (top_now, sum_now) in (
            (query_first, key_first, current[0]),
            (query_second, key_second, current[1]),
        ):
            masked = jnp.where(allowed, scores(query_block, key_block), NEG_FILL)
            top_next = jnp.maximum(top_now, jnp.max(masked, axis=-1))
            fresh = jnp.where(allowed, jnp.exp(masked - top_next[:, :, None]), 0.0)
            result.append((top_next, jnp.sum(fresh, axis=-1)))
        return tuple(result)

    def stats_keep(current):
        return current

    soft_stats = lax.cond(needed(key_docs, jnp.int32(0)), stats_update, stats_keep, stats_init)
    apply_key_first = lax.all_gather(key_one, "sp", axis=0, tiled=True)
    apply_key_second = lax.all_gather(key_two, "sp", axis=0, tiled=True)
    value_block = lax.all_gather(values, "sp", axis=0, tiled=True)
    apply_key_docs = lax.all_gather(documents, "sp", axis=0, tiled=True)

    def apply_update(current):
        allowed = masks(apply_key_docs)
        probs = []
        for query_block, key_block, (top_all, sum_all) in (
            (query_first, apply_key_first, soft_stats[0]),
            (query_second, apply_key_second, soft_stats[1]),
        ):
            raw = scores(query_block, key_block)
            probs.append(
                jnp.where(allowed, jnp.exp(raw - top_all[:, :, None]), 0.0) / sum_all[:, :, None]
            )
        weights = (probs[0] - lambda_col * probs[1]).astype(jnp.bfloat16)
        valued = value_block.reshape(value_block.shape[0], head_count, value_width)
        return current + jnp.einsum(
            "hqk,khv->hqv", weights, valued, preferred_element_type=jnp.float32
        )

    def apply_keep(current):
        return current

    head_out = lax.cond(needed(apply_key_docs, jnp.int32(0)), apply_update, apply_keep, value_init)
    normed_heads = (head_out * rms_scale(head_out, 1e-05) * head_gain * HEAD_SCALE).astype(
        jnp.bfloat16
    )
    attn_rows = normed_heads.transpose(1, 0, 2).reshape(tok_rows, head_count * value_width)
    share_rows = tok_rows // tp_size
    own_start = lax.axis_index("tp") * share_rows
    proj_term = jnp.dot(attn_rows, out_weight, preferred_element_type=jnp.float32)
    projected = lax.psum(proj_term.astype(jnp.bfloat16), "tp").astype(jnp.float32)
    mixed_all = resid.astype(jnp.float32) + projected
    normed_all = (mixed_all * rms_scale(mixed_all, 1e-06) * ffn_gain).astype(jnp.bfloat16)
    mixed_own = lax.dynamic_slice_in_dim(mixed_all, own_start, share_rows, 0)
    route_slots = routes.shape[1]
    capacity = max(2, 2 * tok_rows * route_slots // (seq_size * tp_size))
    assign_total = tok_rows * route_slots
    flat_expert = routes.reshape(assign_total)
    flat_weight = route_weight.reshape(assign_total)
    assign_token = jnp.arange(assign_total, dtype=jnp.int32) // route_slots
    is_mine = flat_expert % tp_size == lax.axis_index("tp")
    target = flat_expert // tp_size
    one_hot = (
        (target[:, None] == jnp.arange(seq_size, dtype=jnp.int32)[None, :]) & is_mine[:, None]
    ).astype(jnp.int32)
    slot_rank = jnp.sum(jnp.cumsum(one_hot, axis=0) * one_hot, axis=1) - 1
    slot_id = jnp.where(is_mine, target * capacity + slot_rank, -1)
    slot_total = seq_size * capacity
    matches = slot_id[None, :] == jnp.arange(slot_total, dtype=jnp.int32)[:, None]
    slot_token = jnp.sum(jnp.where(matches, assign_token[None, :], 0), axis=1)
    slot_live = jnp.any(matches, axis=1)
    outgoing = jnp.where(
        slot_live[:, None], normed_all[slot_token], jnp.zeros((), jnp.bfloat16)
    ).reshape(seq_size, capacity, model_width)
    arrived = lax.all_to_all(outgoing, "sp", split_axis=0, concat_axis=0, tiled=True)
    item_count = arrived.shape[1]
    flat_rows = arrived.reshape(seq_size * item_count, model_width)
    gate_part = jnp.dot(flat_rows, expert_gate[0], preferred_element_type=jnp.float32)
    up_part = jnp.dot(flat_rows, expert_up[0], preferred_element_type=jnp.float32)
    hidden = (jax.nn.silu(gate_part) * up_part).astype(jnp.bfloat16)
    result = jnp.dot(hidden, expert_down[0], preferred_element_type=jnp.float32).astype(
        jnp.bfloat16
    )
    returned = lax.all_to_all(
        result.reshape(seq_size, item_count, model_width),
        "sp",
        split_axis=0,
        concat_axis=0,
        tiled=True,
    )
    returned_flat = returned.reshape(slot_total, model_width)
    picked = returned_flat[jnp.maximum(slot_id, 0)].astype(jnp.float32)
    picked_weight = jnp.where(is_mine, flat_weight, 0.0)
    routed = jnp.sum(
        (picked * picked_weight[:, None]).reshape(tok_rows, route_slots, model_width), axis=1
    )
    shared_act = (
        jax.nn.silu(jnp.dot(normed_all, shared_gate, preferred_element_type=jnp.float32))
        * jnp.dot(normed_all, shared_up, preferred_element_type=jnp.float32)
    ).astype(jnp.bfloat16)
    shared_out = jnp.dot(shared_act, shared_down, preferred_element_type=jnp.float32)
    ffn_own = lax.psum_scatter(
        (routed + shared_out).astype(jnp.bfloat16), "tp", scatter_dimension=0, tiled=True
    ).astype(jnp.float32)
    return (mixed_own + ffn_own).astype(jnp.bfloat16)


def solution(mesh):
    placed = (
        P("sp", None),
        P("sp", "tp"),
        P("sp", "tp"),
        P("sp", "tp"),
        P("sp", "tp"),
        P("sp", "tp"),
        P("sp"),
        P("tp"),
        P(),
        P("tp", None),
        P(),
        P("sp", None),
        P("sp", None),
        P(("sp", "tp"), None, None),
        P(("sp", "tp"), None, None),
        P(("sp", "tp"), None, None),
        P(None, "tp"),
        P(None, "tp"),
        P("tp", None),
    )
    return jax.shard_map(
        local, mesh=mesh, in_specs=placed, out_specs=P(("sp", "tp"), None), check_vma=False
    )
```

profile of v0, /device:TPU:0, one launch (start us, length us, event | category | flops | bytes accessed | tf_op | source)
XLA Modules:
  0.0 388.5 jit_solution(5894218725486632129)
XLA Ops:
  15.9 22.3 %all-gather = s32[8,1,256]{2,1,0:T(1,128)S(1)} all-gather(s32[1,1,256]{2,1,0:T(1,128)S(1)} %bitcast.92), channel_id=1, replica_groups=mesh['sp'=8,'tp'=4] {'sp'}, dimensions={0}, use_global_device_ids=true | all-gather | bytes 9216 | tf_op jit(solution)/shard_map/all_gather | solution.py:94
  42.9 8.6 %all-gather.5.cloned.1.call-done = bf16[2048,256]{0,1:T(8,128)(2,1)} async-done(((bf16[256,256]{0,1:T(8,128)(2,1)}), bf16[2048,256]{0,1:T(8,128)(2,1)}) %all-gather.5.cloned.1.call-update) | async-done | bytes 1048592 | tf_op jit(solution)/shard_map/all_gather | solution.py:91
  51.6 40.5 %all-gather.7.cloned.1.call-done = bf16[2048,256]{0,1:T(8,128)(2,1)} async-done(((bf16[256,256]{0,1:T(8,128)(2,1)}), bf16[2048,256]{0,1:T(8,128)(2,1)}) %all-gather.7.cloned.1.call-update) | async-done | bytes 1048592 | tf_op jit(solution)/shard_map/all_gather | solution.py:71
  92.0 12.4 %conditional.2 = (f32[4,256]{1,0:T(4,128)}, f32[4,256]{1,0:T(4,128)S(1)}, f32[4,256]{1,0:T(4,128)}, f32[4,256]{1,0:T(4,128)S(1)}) conditional(s32[]{:T(128)} %convert_element_type.53, () %tuple.24, (s32[256]{0:T(256)S(1)}, s32[2048]{0:T(1024)S(1)}, s32[256]{0:T(256)S(1)}, bf16[2048,256]{0,1:T(8,128)(2,1)}, bf16[256,4,64]{0,2,1:T(8,128)(2,1)S(1)}, ...), branch_computations={%region_1.0_spmd, %region_2.7_spmd} | conditional | flops 571996160 | bytes 50120764 | solution.py:90
  92.0 2.6 fusion.55
  95.2 3.1 fusion.1
  98.9 5.5 %select_reduce_fusion = (f32[4,256]{1,0:T(4,128)S(1)}, f32[4,256]{1,0:T(4,128)S(1)}) fusion(f32[4,256,2048]{2,1,0:T(8,128)S(1)} %get-tuple-element.106, f32[4,256]{1,0:T(4,128)} %get-tuple-element.122, pred[256,2048]{1,0:T(8,128)(4,1)S(1)} %fusion.2, f32[4,256]{1,0:T(4,128)} %get-tuple-element.120, f32[4,256,2048]{2,1,0:T(8,128)S(1)} %fusion.55), kind=kLoop, calls=%fused_computation.2 | loop fusion | flops 20969472 | bytes 17317888 | tf_op jit(solution)/shard_map/cond/branch_1_fun/reduce_sum | solution.py:84
  104.4 39.0 %all-gather.9.cloned.1.call-done = bf16[2048,512]{0,1:T(8,128)(2,1)} async-done(((bf16[256,512]{0,1:T(8,128)(2,1)}), bf16[2048,512]{0,1:T(8,128)(2,1)}) %all-gather.9.cloned.1.call-update) | async-done | bytes 2097168 | tf_op jit(solution)/shard_map/all_gather | solution.py:93
  143.5 16.7 %conditional.3 = (f32[4,256,128]{1,2,0:T(8,128)S(1)}, f32[4,256,1]{1,0,2:T(4,128)S(1)}) conditional(s32[]{:T(128)} %convert_element_type.53, () %tuple.23, (s32[256]{0:T(256)S(1)}, s32[2048]{0:T(1024)S(1)}, s32[256]{0:T(256)S(1)}, bf16[2048,256]{0,1:T(8,128)(2,1)}, bf16[256,4,64]{0,2,1:T(8,128)(2,1)S(1)}, /*index=5*/f32[4,256]{1,0:T(4,128)}, ...), branch_computations={%region_7.8_spmd, %region_8.0_spmd} | conditional | flops 1098644480 | bytes 22837280 | solution.py:116
  143.5 5.7 %fusion.56 = f32[4,256,2048]{2,1,0:T(8,128)} fusion(bf16[256,4,64]{0,2,1:T(8,128)(2,1)S(1)} %get-tuple-element.58, bf16[2048,4,64]{0,2,1:T(8,128)(2,1)} %bitcast.75), kind=kOutput, calls=%fused_computation.113 | convolution fusion | flops 268435456 | bytes 9568256 | tf_op jit(solution)/shard_map/cond/branch_1_fun/qhd,khd->hqk/dot_general | solution.py:62
  150.6 9.6 %multiply_reduce_fusion = (f32[4,256]{1,0:T(4,128)S(1)}, f32[4,256,128]{1,2,0:T(8,128)S(1)}) fusion(bf16[2048,4,128]{0,2,1:T(8,128)(2,1)} %bitcast.95, f32[4,256,2048]{2,1,0:T(8,128)} %fusion.56, bf16[256,4,64]{0,2,1:T(8,128)(2,1)S(1)} %get-tuple-element.63, bf16[2048,4,64]{0,2,1:T(8,128)(2,1)} %bitcast.82, f32[4,256]{1,0:T(4,128)S(1)} %get-tuple-element.66, ...), kind=kOutput, calls=%fused_computation.21 | convolution fusion | flops 828636160 | bytes 12734480 | tf_op jit(solution)/shard_map/cond/branch_1_fun/hqk,khv->hqv/dot_general | solution.py:109
  160.4 3.4 convolution_convert_fusion.1
  164.6 33.9 %all-reduce.2.cloned.1.call-done = bf16[256,2048]{1,0:T(8,128)(2,1)} async-done(((bf16[256,2048]{1,0:T(8,128)(2,1)}), bf16[256,2048]{1,0:T(8,128)(2,1)}) %all-reduce.2.cloned.1.call-update) | async-done | bytes 1048592 | tf_op jit(solution)/shard_map/psum | solution.py:124
  198.5 3.1 convert_add_fusion
  202.2 3.3 gather_fusion
  207.3 53.2 %all_to_all.10 = bf16[8,64,2048]{2,1,0:T(8,128)(2,1)S(1)} all-to-all(bf16[8,64,2048]{2,1,0:T(8,128)(2,1)S(1)} %broadcast_select_fusion), channel_id=1, replica_groups=mesh['sp'=8,'tp'=4] {'sp'}, dimensions={0} | all-to-all | bytes 4194304 | tf_op jit(solution)/shard_map/all_to_all | solution.py:148
  264.1 6.3 %convolution_convert_fusion = bf16[512,2048]{1,0:T(8,128)(2,1)} fusion(bf16[1,512,2048]{2,1,0:T(8,128)(2,1)S(1)} %copy-done, bf16[512,2048]{1,0:T(8,128)(2,1)} %bitcast.78, bf16[1,2048,512]{2,1,0:T(8,128)(2,1)} %param.37, f32[512,512]{1,0:T(8,128)} %fusion.16), kind=kOutput, calls=%fused_computation.25 | convolution fusion | flops 2150105088 | bytes 9437184 | tf_op jit(solution)/shard_map/dot_general | solution.py:154
  270.3 4.5 %all-to-all-start.1 = ((bf16[8,64,2048]{2,1,0:T(8,128)(2,1)}), bf16[8,64,2048]{2,1,0:T(8,128)(2,1)}, u32[]{:S(2)}, u32[]{:S(2)}) async-start(bf16[8,64,2048]{2,1,0:T(8,128)(2,1)} %bitcast.76), calls=%async_computation.1 | async-start | bytes 4194304 | tf_op jit(solution)/shard_map/all_to_all | solution.py:157
  276.7 45.4 %all-to-all-done.1 = bf16[8,64,2048]{2,1,0:T(8,128)(2,1)} async-done(((bf16[8,64,2048]{2,1,0:T(8,128)(2,1)}), bf16[8,64,2048]{2,1,0:T(8,128)(2,1)}, u32[]{:S(2)}, u32[]{:S(2)}) %all-to-all-start.1) | async-done | bytes 2097184 | tf_op jit(solution)/shard_map/all_to_all | solution.py:157
  322.1 10.7 %gather_fusion.1 = bf16[1024,2048]{1,0:T(8,128)(2,1)} fusion(bf16[512,2048]{1,0:T(8,128)(2,1)} %bitcast.24, s32[1024]{0:T(1024)S(1)} %broadcast_clamp_fusion), kind=kCustom, calls=%fused_computation.1 | custom fusion | bytes 8392704 | tf_op jit(solution)/shard_map/gather | solution.py:165
  332.8 8.3 %reshape.441 = f32[256,4,2048]{2,1,0:T(4,128)} reshape(bf16[1024,2048]{1,0:T(8,128)(2,1)} %gather_fusion.1) | data formatting | bytes 12582912 | tf_op jit(solution)/shard_map/convert_element_type | solution.py:165
  341.1 11.4 %multiply_reduce_fusion.1 = f32[256,2048]{1,0:T(8,128)} fusion(f32[256,4,2048]{2,1,0:T(4,128)} %reshape.441, f32[256,4]{1,0:T(8,128)S(1)} %copy.55), kind=kLoop, calls=%fused_computation.24 | loop fusion | flops 3670016 | bytes 10489856 | tf_op jit(solution)/shard_map/reduce_sum | solution.py:167
  352.5 3.7 fusion.12
  356.2 23.9 %reduce-scatter.2.cloned.1.call-done = bf16[64,2048]{1,0:T(8,128)(2,1)} async-done(((bf16[256,2048]{1,0:T(8,128)(2,1)}), bf16[64,2048]{1,0:T(8,128)(2,1)}) %reduce-scatter.2.cloned.1.call-update) | async-done | bytes 262160 | tf_op jit(solution)/shard_map/reduce_scatter | solution.py:175
  (82 shorter events, 25.2 us)
Async XLA Ops:
  6.5 257.5 %copy-start = (bf16[1,512,2048]{2,1,0:T(8,128)(2,1)S(1)}, bf16[1,512,2048]{2,1,0:T(8,128)(2,1)}, u32[]{:S(2)}) copy-start(bf16[1,512,2048]{2,1,0:T(8,128)(2,1)} %param.38) | copy-start | bytes 6291460
  6.5 7.6 %copy-start.6 = (bf16[256,256]{1,0:T(8,128)(2,1)S(1)}, bf16[256,256]{1,0:T(8,128)(2,1)}, u32[]{:S(2)}) copy-start(bf16[256,256]{1,0:T(8,128)(2,1)} %param.25) | copy-start | bytes 393220
  6.5 8.3 %copy-start.8 = (s32[256]{0:T(256)S(1)}, s32[256]{0:T(256)}, u32[]{:S(2)}) copy-start(s32[256]{0:T(256)} %param.29) | copy-start | bytes 3076
  6.5 45.0 %all-gather.5.cloned.1.call-start = ((), (), s32[]{:S(2)}) async-start(), calls=%async_computation.3 | async-start | bytes 1179648 | tf_op jit(solution)/shard_map/all_gather | solution.py:91
  8.4 83.7 %all-gather.7.cloned.1.call-start = ((), (), s32[]{:S(2)}) async-start(), calls=%async_computation.4 | async-start | bytes 1179648 | tf_op jit(solution)/shard_map/all_gather | solution.py:71
  10.1 133.4 %all-gather.9.cloned.1.call-start = ((), (), s32[]{:S(2)}) async-start(), calls=%async_computation.5 | async-start | bytes 2359296 | tf_op jit(solution)/shard_map/all_gather | solution.py:93
  12.0 186.5 %all-reduce.2.cloned.1.call-start = ((), (), s32[]{:S(2)}) async-start(), calls=%async_computation.6 | async-start | bytes 2097152 | tf_op jit(solution)/shard_map/psum | solution.py:124
  92.0 51.5 %copy-start.13 = (f32[4]{0:T(128)S(1)}, f32[4]{0:T(128)}, u32[]{:S(2)}) copy-start(f32[4]{0:T(128)} %param.30) | copy-start | bytes 52
  92.0 3.2 copy-start.5
  143.5 16.8 %copy-start.11 = (f32[128]{0:T(128)S(1)}, f32[128]{0:T(128)}, u32[]{:S(2)}) copy-start(f32[128]{0:T(128)} %param.31) | copy-start | bytes 1540
  160.4 38.1 %copy-start.1 = (bf16[256,2048]{1,0:T(8,128)(2,1)S(1)}, bf16[256,2048]{1,0:T(8,128)(2,1)}, u32[]{:S(2)}) copy-start(bf16[256,2048]{1,0:T(8,128)(2,1)} %param.23) | copy-start | bytes 3145732
  164.6 37.0 %copy-start.9 = (f32[2048]{0:T(1024)S(1)}, f32[2048]{0:T(1024)}, u32[]{:S(2)}) copy-start(f32[2048]{0:T(1024)} %param.33) | copy-start | bytes 24580
  198.5 3.1 copy-start.2
  198.5 3.1 copy-start.3
  207.3 54.5 %copy-start.12 = (bf16[1,2048,512]{2,1,0:T(8,128)(2,1)S(1)}, bf16[1,2048,512]{2,1,0:T(8,128)(2,1)}, u32[]{:S(2)}) copy-start(bf16[1,2048,512]{2,1,0:T(8,128)(2,1)} %param.36) | copy-start | bytes 6291460
  260.5 1.3 copy-start.4
  270.3 4.7 %copy-start.7 = (s32[256,4]{0,1:T(4,128)S(1)}, s32[256,4]{0,1:T(4,128)}, u32[]{:S(2)}) copy-start(s32[256,4]{0,1:T(4,128)} %param.34) | copy-start | bytes 12292
  270.3 4.7 %copy-start.10 = (f32[256,4]{0,1:T(4,128)S(1)}, f32[256,4]{0,1:T(4,128)}, u32[]{:S(2)}) copy-start(f32[256,4]{0,1:T(4,128)} %param.35) | copy-start | bytes 12292
  270.3 51.7 %all-to-all-start.1 = ((bf16[8,64,2048]{2,1,0:T(8,128)(2,1)}), bf16[8,64,2048]{2,1,0:T(8,128)(2,1)}, u32[]{:S(2)}, u32[]{:S(2)}) async-start(bf16[8,64,2048]{2,1,0:T(8,128)(2,1)} %bitcast.76), calls=%async_computation.1 | async-start | bytes 4194304 | tf_op jit(solution)/shard_map/all_to_all | solution.py:157
  274.8 105.3 %reduce-scatter.2.cloned.1.call-start = ((), (), s32[]{:S(2)}) async-start(), calls=%async_computation.7 | async-start | bytes 1310720 | tf_op jit(solution)/shard_map/reduce_scatter | solution.py:175
Sparse Core Ops, SparseCore 0:
  9.4 42.1 all-gather.4
  53.6 38.3 all-gather.6
  94.1 49.3 all-gather.8
  164.0 34.4 all-reduce.1
  356.3 23.7 reduce-scatter.1
where the time goes:
time: 389 us
  waiting for transfers between devices  191 us (49%)
  blocking collectives  75.5 us (19%)
  matrix products  38.2 us (10%)
  local copies, waits for them, and re-layouts  32.8 us (8%)
  other arithmetic  30.8 us (8%)
  between operations  15.1 us (4%)
  starting transfers between devices  4.67 us (1%)
    all_to_all x1, blocking collectives, local(): lax.all_to_all(outgoing, 'sp', split_axis=0, concat_axis=0, tiled=True)  53.2 us
    all_to_all x1, waiting for transfers between devices, local(): lax.all_to_all(result.reshape(seq_size, item_count, model_width), 'sp', s...  45.4 us
    all_gather x1, waiting for transfers between devices, local(): key_second = lax.all_gather(key_two, 'sp', axis=0, tiled=True)  40.5 us
    all_gather x1, waiting for transfers between devices, local(): value_block = lax.all_gather(values, 'sp', axis=0, tiled=True)  39 us
    psum x1, waiting for transfers between devices, local(): lax.psum(proj_term.astype(jnp.bfloat16), 'tp').astype(jnp.float32)  33.9 us
    reduce_scatter x1, waiting for transfers between devices, local(): lax.psum_scatter((routed + shared_out).astype(jnp.bfloat16), 'tp', scatte...  23.9 us
    all_gather x1, blocking collectives, local(): apply_key_docs = lax.all_gather(documents, 'sp', axis=0, tiled=True)  22.3 us
    dot_general x3, matrix products, scores(): jnp.einsum('qhd,khd->hqk', query_block, keyed, preferred_element_type=jnp...  11.5 us
  transfers between devices with their start and end apart: 6, of which 6 were waited for; matrix products, arithmetic and copies ran while one was open for 6% of the time, Pallas kernels for 0%

commit v1 on v0

--- a/solution.py
+++ b/solution.py
@@ -91,7 +91,9 @@
     apply_key_first = lax.all_gather(key_one, "sp", axis=0, tiled=True)
     apply_key_second = lax.all_gather(key_two, "sp", axis=0, tiled=True)
     value_block = lax.all_gather(values, "sp", axis=0, tiled=True)
-    apply_key_docs = lax.all_gather(documents, "sp", axis=0, tiled=True)
+    apply_key_docs = jnp.concatenate(
+        lax.all_to_all(jnp.stack([documents] * lax.axis_size("sp")), "sp", 0, 0), axis=0
+    )
 
     def apply_update(current):
         allowed = masks(apply_key_docs)

time: 389 us -> 389 us (level)
  waiting for transfers between devices: 191 us -> 183 us
  starting transfers between devices: 4.67 us -> 12 us
    all_gather x1, waiting for transfers between devices: 8.64 us -> 0.11 us  [local(): apply_key_first = lax.all_gather(key_one, 'sp', axis=0, tiled=True)]
    all_to_all x0 -> x1, starting transfers between devices: none -> 7.28 us  [local(): lax.all_to_all(jnp.stack([documents] * lax.axis_size('sp')), 'sp', 0, 0)]
    unnamed x32 -> x34, local copies, waits for them, and re-layouts: 8.52 us -> 7.61 us
  transfers between devices with their start and end apart: 6 -> 7, of which waited for: 6 -> 6; matrix products, arithmetic and copies ran while one was open for 6% -> 7% of each run, Pallas kernels for 0% -> 0%
where the time goes in v1:
time: 389 us; the launch traced here: 388 us
  waiting for transfers between devices  183 us (47%)
  blocking collectives  74.2 us (19%)
  matrix products  38.2 us (10%)
  local copies, waits for them, and re-layouts  33.2 us (9%)
  other arithmetic  31.6 us (8%)
  between operations  16.5 us (4%)
  starting transfers between devices  12 us (3%)
    all_to_all x1, blocking collectives, local(): lax.all_to_all(outgoing, 'sp', split_axis=0, concat_axis=0, tiled=True)  53.2 us
    all_to_all x1, waiting for transfers between devices, local(): lax.all_to_all(result.reshape(seq_size, item_count, model_width), 'sp', s...  45.4 us
    all_gather x1, waiting for transfers between devices, local(): key_second = lax.all_gather(key_two, 'sp', axis=0, tiled=True)  40.3 us
    all_gather x1, waiting for transfers between devices, local(): value_block = lax.all_gather(values, 'sp', axis=0, tiled=True)  39 us
    psum x1, waiting for transfers between devices, local(): lax.psum(proj_term.astype(jnp.bfloat16), 'tp').astype(jnp.float32)  33.9 us
    reduce_scatter x1, waiting for transfers between devices, local(): lax.psum_scatter((routed + shared_out).astype(jnp.bfloat16), 'tp', scatte...  23.9 us
    all_gather x1, blocking collectives, local(): key_docs = lax.all_gather(documents, 'sp', axis=0, tiled=True)  21 us
    dot_general x3, matrix products, scores(): jnp.einsum('qhd,khd->hqk', query_block, keyed, preferred_element_type=jnp...  11.5 us
  transfers between devices with their start and end apart: 7, of which 6 were waited for; matrix products, arithmetic and copies ran while one was open for 7% of the time, Pallas kernels for 0%

profile of v1, /device:TPU:0, one launch (start us, length us, event | category | flops | bytes accessed | tf_op | source)
XLA Modules:
  0.0 388.4 jit_solution(17129593819143572674)
XLA Ops:
  13.3 7.3 %all-to-all-start = ((s32[8,1,256]{2,1,0:T(1,128)}), s32[8,1,256]{2,1,0:T(1,128)S(1)}, u32[]{:S(2)}, u32[]{:S(2)}) async-start(s32[8,1,256]{2,1,0:T(1,128)} %stack.2), calls=%async_computation | async-start | bytes 16384 | tf_op jit(solution)/shard_map/all_to_all | solution.py:95
  26.7 21.0 %all-gather = s32[8,1,256]{2,1,0:T(1,128)S(1)} all-gather(s32[1,1,256]{2,1,0:T(1,128)S(1)} %bitcast.89), channel_id=1, replica_groups=mesh['sp'=8,'tp'=4] {'sp'}, dimensions={0}, use_global_device_ids=true | all-gather | bytes 9216 | tf_op jit(solution)/shard_map/all_gather | solution.py:72
  51.6 40.3 %all-gather.7.cloned.1.call-done = bf16[2048,256]{0,1:T(8,128)(2,1)} async-done(((bf16[256,256]{0,1:T(8,128)(2,1)}), bf16[2048,256]{0,1:T(8,128)(2,1)}) %all-gather.7.cloned.1.call-update) | async-done | bytes 1048592 | tf_op jit(solution)/shard_map/all_gather | solution.py:71
  91.9 12.4 %conditional.2 = (f32[4,256]{1,0:T(4,128)}, f32[4,256]{1,0:T(4,128)S(1)}, f32[4,256]{1,0:T(4,128)}, f32[4,256]{1,0:T(4,128)S(1)}) conditional(s32[]{:T(128)} %convert_element_type.56, () %tuple.24, (s32[256]{0:T(256)S(1)}, s32[2048]{0:T(1024)S(1)}, s32[256]{0:T(256)S(1)}, bf16[2048,256]{0,1:T(8,128)(2,1)}, bf16[256,4,64]{0,2,1:T(8,128)(2,1)S(1)}, ...), branch_computations={%region_2.3_spmd, %region_3.8_spmd} | conditional | flops 571996160 | bytes 50120764 | solution.py:90
  91.9 2.6 fusion.55
  95.1 3.1 fusion.1
  98.8 5.5 %select_reduce_fusion = (f32[4,256]{1,0:T(4,128)S(1)}, f32[4,256]{1,0:T(4,128)S(1)}) fusion(f32[4,256,2048]{2,1,0:T(8,128)S(1)} %get-tuple-element.107, f32[4,256]{1,0:T(4,128)} %get-tuple-element.123, pred[256,2048]{1,0:T(8,128)(4,1)S(1)} %fusion.2, f32[4,256]{1,0:T(4,128)} %get-tuple-element.121, f32[4,256,2048]{2,1,0:T(8,128)S(1)} %fusion.55), kind=kLoop, calls=%fused_computation.2 | loop fusion | flops 20969472 | bytes 17317888 | tf_op jit(solution)/shard_map/cond/branch_1_fun/reduce_sum | solution.py:84
  104.4 39.0 %all-gather.9.cloned.1.call-done = bf16[2048,512]{0,1:T(8,128)(2,1)} async-done(((bf16[256,512]{0,1:T(8,128)(2,1)}), bf16[2048,512]{0,1:T(8,128)(2,1)}) %all-gather.9.cloned.1.call-update) | async-done | bytes 2097168 | tf_op jit(solution)/shard_map/all_gather | solution.py:93
  143.4 16.8 %conditional.3 = (f32[4,256,128]{1,2,0:T(8,128)S(1)}, f32[4,256,1]{1,0,2:T(4,128)S(1)}) conditional(s32[]{:T(128)} %convert_element_type.55, () %tuple.23, (s32[256]{0:T(256)S(1)}, s32[8,1,256]{2,1,0:T(1,128)S(1)}, s32[256]{0:T(256)S(1)}, bf16[2048,256]{0,1:T(8,128)(2,1)}, bf16[256,4,64]{0,2,1:T(8,128)(2,1)S(1)}, /*index=5*/f32[4,256]{1,0:T(4,128)}, ...), branch_computations={%region_8.9_spmd, %region_9.0_spmd} | conditional | flops 1098644480 | bytes 22837280 | solution.py:118
  143.4 5.7 %fusion.56 = f32[4,256,2048]{2,1,0:T(8,128)} fusion(bf16[256,4,64]{0,2,1:T(8,128)(2,1)S(1)} %get-tuple-element.59, bf16[2048,4,64]{0,2,1:T(8,128)(2,1)} %bitcast.76), kind=kOutput, calls=%fused_computation.113 | convolution fusion | flops 268435456 | bytes 9568256 | tf_op jit(solution)/shard_map/cond/branch_1_fun/qhd,khd->hqk/dot_general | solution.py:62
  150.5 9.6 %multiply_reduce_fusion = (f32[4,256]{1,0:T(4,128)S(1)}, f32[4,256,128]{1,2,0:T(8,128)S(1)}) fusion(bf16[2048,4,128]{0,2,1:T(8,128)(2,1)} %bitcast.96, f32[4,256,2048]{2,1,0:T(8,128)} %fusion.56, bf16[256,4,64]{0,2,1:T(8,128)(2,1)S(1)} %get-tuple-element.64, bf16[2048,4,64]{0,2,1:T(8,128)(2,1)} %bitcast.83, f32[4,256]{1,0:T(4,128)S(1)} %get-tuple-element.67, ...), kind=kOutput, calls=%fused_computation.21 | convolution fusion | flops 828636160 | bytes 12734480 | tf_op jit(solution)/shard_map/cond/branch_1_fun/hqk,khv->hqv/dot_general | solution.py:111
  160.3 3.4 convolution_convert_fusion.1
  164.5 33.9 %all-reduce.2.cloned.1.call-done = bf16[256,2048]{1,0:T(8,128)(2,1)} async-done(((bf16[256,2048]{1,0:T(8,128)(2,1)}), bf16[256,2048]{1,0:T(8,128)(2,1)}) %all-reduce.2.cloned.1.call-update) | async-done | bytes 1048592 | tf_op jit(solution)/shard_map/psum | solution.py:126
  198.4 3.1 convert_add_fusion
  202.1 3.3 gather_fusion
  207.2 53.2 %all_to_all.16 = bf16[8,64,2048]{2,1,0:T(8,128)(2,1)S(1)} all-to-all(bf16[8,64,2048]{2,1,0:T(8,128)(2,1)S(1)} %broadcast_select_fusion), channel_id=1, replica_groups=mesh['sp'=8,'tp'=4] {'sp'}, dimensions={0} | all-to-all | bytes 4194304 | tf_op jit(solution)/shard_map/all_to_all | solution.py:150
  263.9 6.3 %convolution_convert_fusion = bf16[512,2048]{1,0:T(8,128)(2,1)} fusion(bf16[1,512,2048]{2,1,0:T(8,128)(2,1)S(1)} %copy-done, bf16[512,2048]{1,0:T(8,128)(2,1)} %bitcast.79, bf16[1,2048,512]{2,1,0:T(8,128)(2,1)} %param.37, f32[512,512]{1,0:T(8,128)} %fusion.16), kind=kOutput, calls=%fused_computation.25 | convolution fusion | flops 2150105088 | bytes 9437184 | tf_op jit(solution)/shard_map/dot_general | solution.py:156
  270.2 4.5 %all-to-all-start.2 = ((bf16[8,64,2048]{2,1,0:T(8,128)(2,1)}), bf16[8,64,2048]{2,1,0:T(8,128)(2,1)}, u32[]{:S(2)}, u32[]{:S(2)}) async-start(bf16[8,64,2048]{2,1,0:T(8,128)(2,1)} %bitcast.77), calls=%async_computation.2 | async-start | bytes 4194304 | tf_op jit(solution)/shard_map/all_to_all | solution.py:159
  276.6 45.4 %all-to-all-done.2 = bf16[8,64,2048]{2,1,0:T(8,128)(2,1)} async-done(((bf16[8,64,2048]{2,1,0:T(8,128)(2,1)}), bf16[8,64,2048]{2,1,0:T(8,128)(2,1)}, u32[]{:S(2)}, u32[]{:S(2)}) %all-to-all-start.2) | async-done | bytes 2097184 | tf_op jit(solution)/shard_map/all_to_all | solution.py:159
  322.0 10.7 %gather_fusion.1 = bf16[1024,2048]{1,0:T(8,128)(2,1)} fusion(bf16[512,2048]{1,0:T(8,128)(2,1)} %bitcast.25, s32[1024]{0:T(1024)S(1)} %broadcast_clamp_fusion), kind=kCustom, calls=%fused_computation.1 | custom fusion | bytes 8392704 | tf_op jit(solution)/shard_map/gather | solution.py:167
  332.6 8.3 %reshape.454 = f32[256,4,2048]{2,1,0:T(4,128)} reshape(bf16[1024,2048]{1,0:T(8,128)(2,1)} %gather_fusion.1) | data formatting | bytes 12582912 | tf_op jit(solution)/shard_map/convert_element_type | solution.py:167
  340.9 11.4 %multiply_reduce_fusion.1 = f32[256,2048]{1,0:T(8,128)} fusion(f32[256,4,2048]{2,1,0:T(4,128)} %reshape.454, f32[256,4]{1,0:T(8,128)S(1)} %copy.55), kind=kLoop, calls=%fused_computation.24 | loop fusion | flops 3670016 | bytes 10489856 | tf_op jit(solution)/shard_map/reduce_sum | solution.py:169
  352.4 3.7 fusion.12
  356.1 23.9 %reduce-scatter.2.cloned.1.call-done = bf16[64,2048]{1,0:T(8,128)(2,1)} async-done(((bf16[256,2048]{1,0:T(8,128)(2,1)}), bf16[64,2048]{1,0:T(8,128)(2,1)}) %reduce-scatter.2.cloned.1.call-update) | async-done | bytes 262160 | tf_op jit(solution)/shard_map/reduce_scatter | solution.py:177
  (88 shorter events, 26.6 us)
Async XLA Ops:
  6.5 257.4 %copy-start = (bf16[1,512,2048]{2,1,0:T(8,128)(2,1)S(1)}, bf16[1,512,2048]{2,1,0:T(8,128)(2,1)}, u32[]{:S(2)}) copy-start(bf16[1,512,2048]{2,1,0:T(8,128)(2,1)} %param.38) | copy-start | bytes 6291460
  6.5 18.1 %copy-start.8 = (s32[256]{0:T(256)S(1)}, s32[256]{0:T(256)}, u32[]{:S(2)}) copy-start(s32[256]{0:T(256)} %param.29) | copy-start | bytes 3076
  6.5 18.6 %copy-start.6 = (bf16[256,256]{1,0:T(8,128)(2,1)S(1)}, bf16[256,256]{1,0:T(8,128)(2,1)}, u32[]{:S(2)}) copy-start(bf16[256,256]{1,0:T(8,128)(2,1)} %param.25) | copy-start | bytes 393220
  6.5 18.7 %copy-start.7 = (bf16[256,256]{1,0:T(8,128)(2,1)S(1)}, bf16[256,256]{1,0:T(8,128)(2,1)}, u32[]{:S(2)}) copy-start(bf16[256,256]{1,0:T(8,128)(2,1)} %param.24) | copy-start | bytes 393220
  6.5 45.1 %all-gather.5.cloned.1.call-start = ((), (), s32[]{:S(2)}) async-start(), calls=%async_computation.4 | async-start | bytes 1179648 | tf_op jit(solution)/shard_map/all_gather | solution.py:91
  8.4 83.5 %all-gather.7.cloned.1.call-start = ((), (), s32[]{:S(2)}) async-start(), calls=%async_computation.5 | async-start | bytes 1179648 | tf_op jit(solution)/shard_map/all_gather | solution.py:71
  10.1 133.2 %all-gather.9.cloned.1.call-start = ((), (), s32[]{:S(2)}) async-start(), calls=%async_computation.6 | async-start | bytes 2359296 | tf_op jit(solution)/shard_map/all_gather | solution.py:93
  13.3 36.3 %all-to-all-start = ((s32[8,1,256]{2,1,0:T(1,128)}), s32[8,1,256]{2,1,0:T(1,128)S(1)}, u32[]{:S(2)}, u32[]{:S(2)}) async-start(s32[8,1,256]{2,1,0:T(1,128)} %stack.2), calls=%async_computation | async-start | bytes 16384 | tf_op jit(solution)/shard_map/all_to_all | solution.py:95
  20.6 177.8 %all-reduce.2.cloned.1.call-start = ((), (), s32[]{:S(2)}) async-start(), calls=%async_computation.7 | async-start | bytes 2097152 | tf_op jit(solution)/shard_map/psum | solution.py:126
  91.9 51.5 %copy-start.14 = (f32[4]{0:T(128)S(1)}, f32[4]{0:T(128)}, u32[]{:S(2)}) copy-start(f32[4]{0:T(128)} %param.30) | copy-start | bytes 52
  91.9 3.2 copy-start.5
  143.4 16.8 %copy-start.12 = (f32[128]{0:T(128)S(1)}, f32[128]{0:T(128)}, u32[]{:S(2)}) copy-start(f32[128]{0:T(128)} %param.31) | copy-start | bytes 1540
  160.3 38.1 %copy-start.1 = (bf16[256,2048]{1,0:T(8,128)(2,1)S(1)}, bf16[256,2048]{1,0:T(8,128)(2,1)}, u32[]{:S(2)}) copy-start(bf16[256,2048]{1,0:T(8,128)(2,1)} %param.23) | copy-start | bytes 3145732
  164.5 37.0 %copy-start.10 = (f32[2048]{0:T(1024)S(1)}, f32[2048]{0:T(1024)}, u32[]{:S(2)}) copy-start(f32[2048]{0:T(1024)} %param.33) | copy-start | bytes 24580
  198.4 3.1 copy-start.2
  198.4 3.1 copy-start.3
  207.2 54.5 %copy-start.13 = (bf16[1,2048,512]{2,1,0:T(8,128)(2,1)S(1)}, bf16[1,2048,512]{2,1,0:T(8,128)(2,1)}, u32[]{:S(2)}) copy-start(bf16[1,2048,512]{2,1,0:T(8,128)(2,1)} %param.36) | copy-start | bytes 6291460
  260.4 1.3 copy-start.4
  270.2 4.7 %copy-start.9 = (s32[256,4]{0,1:T(4,128)S(1)}, s32[256,4]{0,1:T(4,128)}, u32[]{:S(2)}) copy-start(s32[256,4]{0,1:T(4,128)} %param.34) | copy-start | bytes 12292
  270.2 4.7 %copy-start.11 = (f32[256,4]{0,1:T(4,128)S(1)}, f32[256,4]{0,1:T(4,128)}, u32[]{:S(2)}) copy-start(f32[256,4]{0,1:T(4,128)} %param.35) | copy-start | bytes 12292
  270.2 51.7 %all-to-all-start.2 = ((bf16[8,64,2048]{2,1,0:T(8,128)(2,1)}), bf16[8,64,2048]{2,1,0:T(8,128)(2,1)}, u32[]{:S(2)}, u32[]{:S(2)}) async-start(bf16[8,64,2048]{2,1,0:T(8,128)(2,1)} %bitcast.77), calls=%async_computation.2 | async-start | bytes 4194304 | tf_op jit(solution)/shard_map/all_to_all | solution.py:159
  274.7 105.2 %reduce-scatter.2.cloned.1.call-start = ((), (), s32[]{:S(2)}) async-start(), calls=%async_computation.8 | async-start | bytes 1310720 | tf_op jit(solution)/shard_map/reduce_scatter | solution.py:177
Sparse Core Ops, SparseCore 0:
  9.4 42.2 all-gather.4
  53.7 38.2 all-gather.6
  94.0 49.3 all-gather.8
  163.9 34.4 all-reduce.1
  356.2 23.7 reduce-scatter.1
